TPU v7x, 32 devices: a whole 2x2x4 slice. The times are simulated.
32 devices in a mesh: grp: 2 (over y), sp: 4 (over z), tp: 4 (over x, core).
Axes of the slice: x: 2, y: 2, z: 4, core: 2. Of those that a mesh axis runs over, the one named last changes fastest.
Arguments:
- recept: bfloat16 [4096, 2048], P(('grp', 'sp'), 'tp'), parts along dimension 0, may hold values from -6 to 6
- key_input: bfloat16 [4096, 2048], P(('grp', 'sp'), 'tp'), parts along dimension 0, may hold values from -6 to 6
- value_input: bfloat16 [4096, 2048], P(('grp', 'sp'), 'tp'), parts along dimension 0, may hold values from -6 to 6
- output_gate_input: bfloat16 [4096, 2048], P(('grp', 'sp'), 'tp'), parts along dimension 0, may hold values from -6 to 6
- decay_input_part: bfloat16 [4096, 2048], P(('grp', 'sp'), 'tp'), parts along dimension 0, may hold values from -4.8 to 4.8
- correction_rate_input: bfloat16 [4096, 2048], P(('grp', 'sp'), 'tp'), parts along dimension 0, may hold values from -4 to 4
- head_decay_offset: float32 [4096, 32], P(('grp', 'sp'), 'tp'), parts along dimension 0, may hold values from -2.1 to 0
- decay_fixed_bias: float32 [2048], P('tp'), may hold values from -11.5 to -2.8
- correction_rate_bias: float32 [2048], P('tp'), may hold values from -8.5 to 1
- head_norm_gain: float32 [2048], P('tp'), may hold values from 0.1 to 1.9
- self_term_weight: float32 [2048], P('tp'), may hold values from -2 to 2
- output_weight_matrix: bfloat16 [2048, 2048], P('tp'), may hold values from -0.125 to 0.125
- residual: bfloat16 [4096, 2048], P(('grp', 'sp', 'tp')), parts along dimension 0, may hold values from -6 to 6
- feedforward_norm_gain: float32 [2048], replicated, may hold values from 0.1 to 1.9
- routed_expert_index: int32 [4096, 2], P(('grp', 'sp', 'tp')), parts along dimension 0, may hold values from 0 to 3, all different within a row; in each aligned block of 128 rows (0 to 127, 128 to 255, ...) at most 96 rows name the same one
- routed_expert_weight: float32 [4096, 2], P(('grp', 'sp', 'tp')), parts along dimension 0, may hold values from 0.2 to 1
- gate_weight_experts: bfloat16 [4, 2048, 1024], P('sp', None, 'tp'), may hold values from -0.125 to 0.125
- up_weight_experts: bfloat16 [4, 2048, 1024], P('sp', None, 'tp'), may hold values from -0.125 to 0.125
- down_weight_experts: bfloat16 [4, 1024, 2048], P('sp', 'tp'), may hold values from -0.1875 to 0.1875
Outputs:
- output: bfloat16 [4096, 2048], P(('grp', 'sp', 'tp')), parts along dimension 0
There are 2 independent parts, one for each index of `grp`. A program takes and returns all parts, laid end to end along the dimension named above; an argument that names none is the same for every part. Nothing has to cross between parts.
Inputs may be any that keep to these rules, and one draw needn't show every extreme that they name: `routed_expert_index`: in each aligned block of 128 rows (the rows of one device) no expert is named by more than 96 routes; the two experts of a row differ.
All inputs are finite; a program needn't handle non-finite values.
Results may differ from a plain program's by a relative error of at most 0.0058.
Values may be sent and summed in bfloat16 or wider, within the bound.
No kernel may reach another device: no remote copies, remote signals or barrier semaphores. Data moves between devices by JAX's collectives and lax.ppermute only.
A program may use at most 128 MiB of HBM per device.

v0:
```python
import jax
import jax.numpy as jnp
from jax import lax
from jax.sharding import PartitionSpec as P

SPAN = 64


PRECISE = lax.Precision.HIGHEST
GROUP_EPS = 0.00064
NORM_EPS = 1e-06


def prefix_2(part, axis, combine, identity):
    place = lax.axis_index(axis)
    gathered = jax.tree.map(lambda a: lax.all_gather(a, axis), part)
    state = jax.tree.map(lambda a, e: jnp.zeros_like(a) + jnp.asarray(e, a.dtype), part, identity)

    def one(lap, state):
        return combine(
            state, jax.tree.map(lambda a: lax.dynamic_index_in_dim(a, lap, 0, False), gathered)
        )

    return lax.fori_loop(0, place, one, state)


def chain_combine(earlier, later):
    transit = jnp.einsum("hij,hjk->hik", earlier[0], later[0], precision=PRECISE)
    carried = jnp.einsum("hij,hjk->hik", earlier[1], later[0], precision=PRECISE) + later[1]
    return (transit, carried)


def pair_scores(left, right):
    return jnp.einsum("bhtn,bhsn->bhts", left, right, precision=PRECISE)


def apply_scores(left, right):
    return jnp.einsum("bhts,bhsn->bhtn", left, right, precision=PRECISE)


def outer_sum(left, right):
    return jnp.einsum("bhtn,bhtm->bhnm", left, right, precision=PRECISE)


def square_blocks(left, right):
    return jnp.einsum("bhts,bhsu->bhtu", left, right, precision=PRECISE)


def unit_lower_inverse(strict_lower, span):
    inverse = jnp.eye(span, dtype=jnp.float32) + strict_lower
    power = strict_lower
    for level in range(1, (span - 1).bit_length()):
        power = square_blocks(power, power)
        inverse = inverse + square_blocks(power, inverse)
    return inverse


def mixer(
    recept,
    key_input,
    value_input,
    output_gate_input,
    decay_input_part,
    correction_rate_input,
    head_decay_offset,
    decay_fixed_bias,
    correction_rate_bias,
    head_norm_gain,
    self_term_weight,
    span,
):
    sequence_length, channel_width = recept.shape
    head_split = head_decay_offset.shape[1]
    head_width = channel_width // head_split
    blocks = sequence_length // span

    def split_heads(tensor):
        return (
            tensor.astype(jnp.float32)
            .reshape(blocks, span, head_split, head_width)
            .transpose(0, 2, 1, 3)
        )

    weight_logarithm = (
        -jax.nn.softplus(-(decay_fixed_bias + decay_input_part.astype(jnp.float32))) - 0.5
    )
    decay_logarithm = (
        -jnp.exp(weight_logarithm).reshape(sequence_length, head_split, head_width)
        + head_decay_offset[:, :, None]
    )
    decay_logarithm = split_heads(decay_logarithm.reshape(sequence_length, channel_width))
    rate = split_heads(
        jax.nn.sigmoid(correction_rate_bias + correction_rate_input.astype(jnp.float32))
    )
    receptance_per_head, key_per_head, value_per_head = (
        split_heads(recept),
        split_heads(key_input),
        split_heads(value_input),
    )
    unit_key = key_per_head * lax.rsqrt(
        jnp.sum(key_per_head * key_per_head, axis=-1, keepdims=True) + NORM_EPS
    )
    remove_vec = -unit_key
    write_vec = unit_key * rate
    cumul = jnp.cumsum(decay_logarithm, axis=2)
    remove_til = remove_vec * jnp.exp(cumul - decay_logarithm)
    recept_til = receptance_per_head * jnp.exp(cumul)
    write_hat = write_vec * jnp.exp(-cumul)
    key_hat = key_per_head * jnp.exp(-cumul)
    ending = jnp.exp(cumul[:, :, -1:, :])
    offsets = jnp.arange(span, dtype=jnp.int32)
    strict = offsets[:, None] > offsets[None, :]
    within = offsets[:, None] >= offsets[None, :]
    remove_write = jnp.where(strict, pair_scores(remove_til, write_hat), 0.0)
    remove_key = jnp.where(strict, pair_scores(remove_til, key_hat), 0.0)
    read_write = jnp.where(within, pair_scores(recept_til, write_hat), 0.0)
    read_key = jnp.where(within, pair_scores(recept_til, key_hat), 0.0)
    inverse = unit_lower_inverse(remove_write, span)
    inv_remove = apply_scores(inverse, remove_til)
    inv_value = apply_scores(inverse, apply_scores(remove_key, value_per_head))
    read_map = recept_til + apply_scores(read_write, inv_remove)
    read_own = apply_scores(read_write, inv_value) + apply_scores(read_key, value_per_head)
    write_end = write_hat * ending
    key_end = key_hat * ending
    eye_head = jnp.eye(head_width, dtype=jnp.float32)
    transit = outer_sum(inv_remove, write_end) + eye_head * ending[:, :, 0, None, :]
    added = outer_sum(inv_value, write_end) + outer_sum(value_per_head, key_end)
    identity = jnp.broadcast_to(eye_head, (head_split, head_width, head_width))
    zero_state = jnp.zeros((head_split, head_width, head_width), jnp.float32)

    def block_step(carry, inputs):
        return (chain_combine(carry, inputs), carry)

    device_total, block_starts = lax.scan(block_step, (identity, zero_state), (transit, added))
    prefix = prefix_2(device_total, "sp", chain_combine, (identity, zero_state))
    entering = prefix[1]
    true_start = (
        jnp.einsum("hvk,bhkm->bhvm", entering, block_starts[0], precision=PRECISE) + block_starts[1]
    )
    readout = jnp.einsum("bhtk,bhvk->bhtv", read_map, true_start, precision=PRECISE) + read_own
    center = jnp.mean(readout, axis=-1, keepdims=True)
    spread = jnp.mean(jnp.square(readout - center), axis=-1, keepdims=True)
    gains = head_norm_gain.reshape(head_split, head_width)[None, :, None, :]
    normalized_state = (readout - center) * lax.rsqrt(spread + GROUP_EPS) * gains
    self_term_head = self_term_weight.reshape(head_split, head_width)[None, :, None, :]
    self_term = (
        jnp.sum(receptance_per_head * key_per_head * self_term_head, axis=-1, keepdims=True)
        * value_per_head
    )
    merged_heads = (
        (normalized_state + self_term).transpose(0, 2, 1, 3).reshape(sequence_length, channel_width)
    )
    return (merged_heads * output_gate_input.astype(jnp.float32)).astype(jnp.bfloat16)


def local(
    recept,
    key_input,
    value_input,
    output_gate_input,
    decay_input_part,
    correction_rate_input,
    head_decay_offset,
    decay_fixed_bias,
    correction_rate_bias,
    head_norm_gain,
    self_term_weight,
    output_weight_matrix,
    residual,
    feedforward_norm_gain,
    routed_expert_index,
    routed_expert_weight,
    gate_weight_experts,
    up_weight_experts,
    down_weight_experts,
):
    attention_result = mixer(
        recept,
        key_input,
        value_input,
        output_gate_input,
        decay_input_part,
        correction_rate_input,
        head_decay_offset,
        decay_fixed_bias,
        correction_rate_bias,
        head_norm_gain,
        self_term_weight,
        SPAN,
    )
    proj = lax.psum_scatter(
        jnp.dot(attention_result, output_weight_matrix, preferred_element_type=jnp.float32),
        "tp",
        scatter_dimension=0,
        tiled=True,
    )
    proj = proj.astype(jnp.bfloat16)
    stream = residual.astype(jnp.float32) + lax.optimization_barrier(proj).astype(jnp.float32)
    ffn_in = (
        stream
        * lax.rsqrt(jnp.mean(stream * stream, axis=-1, keepdims=True) + NORM_EPS)
        * feedforward_norm_gain
    ).astype(jnp.bfloat16)
    local_rows = ffn_in.shape[0]
    top_count = routed_expert_index.shape[1]
    experts = gate_weight_experts.shape[0] * lax.axis_size("sp")
    capacity = max(2, 3 * local_rows // experts)
    flat_ids = routed_expert_index.reshape(-1)
    hits = (flat_ids[:, None] == jnp.arange(experts, dtype=jnp.int32)[None, :]).astype(jnp.int32)
    earlier_hits = jnp.cumsum(hits, axis=0) - hits
    slot_index = jnp.sum(earlier_hits * hits, axis=1)
    target = flat_ids * capacity + slot_index
    places = (target[:, None] == jnp.arange(experts * capacity, dtype=jnp.int32)[None, :]).astype(
        jnp.bfloat16
    )
    places = jnp.sum(places.reshape(local_rows, top_count, experts * capacity), axis=1)
    outgoing = jnp.einsum("rs,rd->sd", places, ffn_in, preferred_element_type=jnp.float32)
    outgoing = outgoing.astype(jnp.bfloat16).reshape(experts, capacity, ffn_in.shape[1])
    incoming = lax.all_gather(
        lax.all_to_all(outgoing, "sp", split_axis=0, concat_axis=0, tiled=True),
        "tp",
        axis=0,
        tiled=True,
    )
    flat = incoming.reshape(-1, incoming.shape[-1])
    gated = jnp.dot(flat, gate_weight_experts[0], preferred_element_type=jnp.float32)
    upward = jnp.dot(flat, up_weight_experts[0], preferred_element_type=jnp.float32)
    hidden = (jax.nn.silu(gated) * upward).astype(jnp.bfloat16)
    result = jnp.dot(hidden, down_weight_experts[0], preferred_element_type=jnp.float32)
    spread_rows = lax.optimization_barrier(
        result.astype(jnp.bfloat16).reshape(incoming.shape)
    ).astype(jnp.float32)
    summed = lax.psum_scatter(
        spread_rows.astype(jnp.bfloat16), "tp", scatter_dimension=0, tiled=True
    )
    expert_out = lax.all_to_all(summed, "sp", split_axis=0, concat_axis=0, tiled=True)
    table = expert_out.reshape(experts * capacity, expert_out.shape[-1])
    fetched = jnp.take(table, target, axis=0).astype(jnp.float32)
    weighted = jnp.sum(
        fetched.reshape(local_rows, top_count, -1) * routed_expert_weight[:, :, None], axis=1
    )
    return (stream + weighted).astype(jnp.bfloat16)


def solution(mesh):
    return jax.shard_map(
        local,
        mesh=mesh,
        in_specs=(
            P(("grp", "sp"), "tp"),
            P(("grp", "sp"), "tp"),
            P(("grp", "sp"), "tp"),
            P(("grp", "sp"), "tp"),
            P(("grp", "sp"), "tp"),
            P(("grp", "sp"), "tp"),
            P(("grp", "sp"), "tp"),
            P("tp"),
            P("tp"),
            P("tp"),
            P("tp"),
            P("tp", None),
            P(("grp", "sp", "tp"), None),
            P(),
            P(("grp", "sp", "tp"), None),
            P(("grp", "sp", "tp"), None),
            P("sp", None, "tp"),
            P("sp", None, "tp"),
            P("sp", "tp", None),
        ),
        out_specs=P(("grp", "sp", "tp"), None),
        check_vma=False,
    )
```

profile of v0, /device:TPU:0, one launch (start us, length us, event | category | flops | bytes accessed | tf_op | source)
XLA Modules:
  0.0 529.3 jit_solution(16448836899378870690)
XLA Ops:
  18.8 3.9 fusion.23
  24.8 6.1 %fusion.20 = (f32[8,8,64,64]{3,2,1,0:T(8,128)S(1)}, f32[8,8,64,64]{3,2,1,0:T(8,128)S(1)}) fusion(f32[8,64,8,64]{3,2,1,0:T(8,128)} %reshape.157, f32[8,8,64,64]{3,1,2,0:T(8,128)} %fusion.24, f32[8,64,8,64]{3,2,1,0:T(8,128)} %reshape.168, f32[8,8,64]{2,1,0:T(8,128)S(1)} %add_rsqrt_fusion, f32[8,64,8]{1,2,0:T(8,128)S(1)} %copy.161, f32[8,64,8,64]{3,2,1,0:T(8,128)} %neg.35), kind=kLoop, calls=%fused_computation.36 | loop fusion | flops 2097152 | bytes 6324224 | tf_op jit(solution)/shard_map/mul | solution.py:108
  31.0 5.4 %fusion.106 = f32[8,8,64,64]{3,2,1,0:T(8,128)} fusion(f32[8,8,64,64]{3,2,1,0:T(8,128)S(1)} %get-tuple-element.199, f32[8,8,64,64]{3,1,2,0:T(8,128)S(1)} %copy-done.1, f32[8,64,8,64]{3,2,1,0:T(8,128)S(1)} %copy-done.4), kind=kOutput, calls=%fused_computation.153 | convolution fusion | flops 201850880 | bytes 4194304 | tf_op jit(solution)/shard_map/bhtn,bhsn->bhts/dot_general | solution.py:34
  39.9 5.3 %fusion.105 = f32[8,8,64,64]{3,2,1,0:T(8,128)} fusion(f32[8,8,64,64]{3,2,1,0:T(8,128)S(1)} %get-tuple-element.198, f32[8,64,8,64]{3,2,1,0:T(8,128)S(1)} %copy-done.6, f32[8,8,64,64]{3,1,2,0:T(8,128)S(1)} %copy-done.1), kind=kOutput, calls=%fused_computation.152 | convolution fusion | flops 201588736 | bytes 4194304 | tf_op jit(solution)/shard_map/bhtn,bhsn->bhts/dot_general | solution.py:34
  47.7 3.6 fusion.110
  51.2 3.8 add_add_fusion.1
  55.1 9.7 %fusion.104 = f32[8,8,64,64]{3,2,1,0:T(8,128)} fusion(f32[8,64,8,64]{3,2,1,0:T(8,128)} %reshape.167, f32[8,8,64,64]{3,1,2,0:T(8,128)} %fusion.24, f32[8,64,8,64]{3,2,1,0:T(8,128)} %reshape.168), kind=kOutput, calls=%fused_computation.151 | convolution fusion | flops 202113024 | bytes 4194304 | tf_op jit(solution)/shard_map/bhtn,bhsn->bhts/dot_general | solution.py:34
  74.7 3.6 fusion.115
  78.2 3.8 fusion.114
  87.0 5.5 %convolution_add_fusion = f32[8,8,64,64]{3,2,1,0:T(8,128)S(1)} fusion(f32[8,8,64,64]{3,2,1,0:T(8,128)} %fusion.115, f32[8,8,64,64]{3,2,1,0:T(8,128)} %copy-done.16, f32[8,8,64,64]{3,2,1,0:T(8,128)} %fusion.114), kind=kOutput, calls=%fused_computation.77 | convolution fusion | flops 201850880 | bytes 4194304 | tf_op jit(solution)/shard_map/bhts,bhsu->bhtu/dot_general | solution.py:46
  96.6 3.7 fusion.117
  102.3 5.2 multiply_add_fusion
  107.5 3.6 fusion.47
  111.1 4.9 fusion.45
  116.0 3.6 bitcast_add_fusion.2
  119.6 54.2 %while.30 = (s32[]{:T(128)}, f32[8,64,64]{1,2,0:T(8,128)S(1)}, f32[8,64,64]{1,2,0:T(8,128)}, f32[8,8,64,64]{2,3,1,0:T(8,128)}, f32[8,8,64,64]{2,3,1,0:T(8,128)},...) while((s32[]{:T(128)}, f32[8,64,64]{1,2,0:T(8,128)S(1)}, ...), condition=%wide.region_3.4_spmd.clone, body=%wide.region_2.3_spmd.clone.sunk | while | flops 50429952 | bytes 3016300 | solution.py:134
  173.9 24.6 %all-gather = f32[32,64,64]{2,1,0:T(8,128)} all-gather(f32[8,64,64]{2,1,0:T(8,128)S(1)} %copy.180), channel_id=2, replica_groups=mesh['grp'=2,'sp'=4,'tp'=4] {'sp'}, dimensions={0}, use_global_device_ids=true | all-gather | bytes 655360 | tf_op jit(solution)/shard_map/all_gather | solution.py:16
  199.6 21.8 %all-gather.1 = f32[32,64,64]{2,1,0:T(8,128)} all-gather(f32[8,64,64]{2,1,0:T(8,128)S(1)} %copy.181), channel_id=3, replica_groups=mesh['grp'=2,'sp'=4,'tp'=4] {'sp'}, dimensions={0}, use_global_device_ids=true | all-gather | bytes 655360 | tf_op jit(solution)/shard_map/all_gather | solution.py:16
  221.5 3.7 fusion.87
  225.3 6.7 %fusion.19 = f32[8,8,64,64]{2,3,1,0:T(8,128)S(1)} fusion(f32[8,8,64,64]{2,3,1,0:T(8,128)} %get-tuple-element.93, f32[8,8,64,64]{3,2,0,1:T(8,128)S(1)} %fusion.87, f32[8,8,64,64]{3,2,1,0:T(8,128)} %fusion.47, f32[8,64,8,64]{3,2,1,0:T(8,128)S(1)} %copy-done.7, f32[8,8,64,64]{3,1,2,0:T(8,128)S(1)} %copy-done.3), kind=kOutput, calls=%fused_computation.33 | convolution fusion | flops 202113024 | bytes 6291456 | tf_op jit(solution)/shard_map/bhtk,bhvk->bhtv/dot_general | solution.py:140
  236.0 3.5 fusion.18
  244.5 4.3 fusion.83
  251.9 48.6 %reduce-scatter.3.cloned.1.call-done = f32[128,2048]{1,0:T(8,128)} async-done(((f32[512,2048]{1,0:T(8,128)}), f32[128,2048]{1,0:T(8,128)}) %reduce-scatter.3.cloned.1.call-update) | async-done | bytes 1048592 | tf_op jit(solution)/shard_map/reduce_scatter | solution.py:191
  302.7 41.3 %all_to_all.10 = bf16[4,96,2048]{2,1,0:T(8,128)(2,1)} all-to-all(bf16[4,96,2048]{2,1,0:T(8,128)(2,1)S(1)} %bitcast.191), channel_id=1, replica_groups=mesh['grp'=2,'sp'=4,'tp'=4] {'sp'}, dimensions={0} | all-to-all | bytes 3145728 | tf_op jit(solution)/shard_map/all_to_all | solution.py:220
  344.1 44.6 %all-gather.4.cloned.1.call-done = bf16[16,96,2048]{2,1,0:T(8,128)(2,1)} async-done(((bf16[4,96,2048]{2,1,0:T(8,128)(2,1)}), bf16[16,96,2048]{2,1,0:T(8,128)(2,1)}) %all-gather.4.cloned.1.call-update) | async-done | bytes 6291472 | tf_op jit(solution)/shard_map/all_gather | solution.py:219
  388.7 6.0 %fusion.64 = f32[1536,256]{1,0:T(8,128)} fusion(bf16[1536,2048]{1,0:T(8,128)(2,1)} %bitcast.198, bf16[1,2048,256]{2,1,0:T(8,128)(2,1)} %param.39), kind=kOutput, calls=%fused_computation.87 | convolution fusion | flops 1610612736 | bytes 8912896 | tf_op jit(solution)/shard_map/dot_general | solution.py:226
  394.7 12.8 %convolution_convert_fusion = bf16[1536,2048]{1,0:T(8,128)(2,1)} fusion(bf16[1536,2048]{1,0:T(8,128)(2,1)} %bitcast.199, f32[1536,256]{1,0:T(8,128)} %fusion.64, bf16[1,256,2048]{2,1,0:T(8,128)(2,1)} %param.41, bf16[1,2048,256]{2,1,0:T(8,128)(2,1)} %param.40), kind=kOutput, calls=%fused_computation.23 | convolution fusion | flops 3226730496 | bytes 16252928 | tf_op jit(solution)/shard_map/dot_general | solution.py:229
  407.6 59.0 %reduce-scatter.5.cloned.1.call-done = bf16[4,96,2048]{2,1,0:T(8,128)(2,1)} async-done(((bf16[16,96,2048]{2,1,0:T(8,128)(2,1)}), bf16[4,96,2048]{2,1,0:T(8,128)(2,1)}) %reduce-scatter.5.cloned.1.call-update) | async-done | bytes 1572880 | tf_op jit(solution)/shard_map/reduce_scatter | solution.py:233
  466.6 4.9 all-to-all-start.1
  472.0 36.3 %all-to-all-done.1 = bf16[4,96,2048]{2,1,0:T(8,128)(2,1)} async-done(((bf16[4,96,2048]{2,1,0:T(8,128)(2,1)}), bf16[4,96,2048]{2,1,0:T(8,128)(2,1)}, u32[]{:S(2)}, u32[]{:S(2)}) %all-to-all-start.1) | async-done | bytes 1572896 | tf_op jit(solution)/shard_map/all_to_all | solution.py:236
  508.4 5.0 gather_fusion
  515.9 5.5 %multiply_reduce_fusion = f32[128,2048]{1,0:T(8,128)S(1)} fusion(bf16[128,2,2048]{2,1,0:T(2,128)(2,1)} %gather.7, pred[128,2]{1,0:T(8,128)(4,1)S(1)} %copy.195, f32[128,2]{1,0:T(8,128)S(1)} %copy.197), kind=kLoop, calls=%fused_computation.49 | loop fusion | flops 1835008 | bytes 2098432 | tf_op jit(solution)/shard_map/reduce_sum | solution.py:239
  (204 shorter events, 114.0 us)
Async XLA Ops:
  6.5 238.0 %copy-start = (bf16[512,2048]{1,0:T(8,128)(2,1)S(1)}, bf16[512,2048]{1,0:T(8,128)(2,1)}, u32[]{:S(2)}) copy-start(bf16[512,2048]{1,0:T(8,128)(2,1)} %param.34) | copy-start | bytes 6291460
  6.5 294.0 %reduce-scatter.3.cloned.1.call-start = ((), (), s32[]{:S(2)}) async-start(), calls=%async_computation.4 | async-start | bytes 5242880 | tf_op jit(solution)/shard_map/reduce_scatter | solution.py:191
  6.6 3.8 copy-start.28
  12.6 2.6 copy-start.25
  15.2 3.6 copy-start.32
  18.8 3.9 copy-start.27
  18.8 3.9 copy-start.31
  24.8 6.2 %copy-start.1 = (f32[8,8,64,64]{3,1,2,0:T(8,128)S(1)}, f32[8,8,64,64]{3,1,2,0:T(8,128)}, u32[]{:S(2)}) copy-start(f32[8,8,64,64]{3,1,2,0:T(8,128)} %fusion.24) | copy-start | bytes 3145732
  24.8 6.2 %copy-start.4 = (f32[8,64,8,64]{3,2,1,0:T(8,128)S(1)}, f32[8,64,8,64]{3,2,1,0:T(8,128)}, u32[]{:S(2)}) copy-start(f32[8,64,8,64]{3,2,1,0:T(8,128)} %reshape.168) | copy-start | bytes 3145732
  31.0 5.4 %copy-start.11 = (f32[8,8,64,64]{3,2,1,0:T(8,128)}, f32[8,8,64,64]{3,2,1,0:T(8,128)S(1)}, u32[]{:S(2)}) copy-start(f32[8,8,64,64]{3,2,1,0:T(8,128)S(1)} %get-tuple-element.199) | copy-start | bytes 3145732
  31.0 8.9 %copy-start.8 = (f32[8,8,64,64]{3,2,1,0:T(8,128)}, f32[8,8,64,64]{3,2,1,0:T(8,128)S(1)}, u32[]{:S(2)}) copy-start(f32[8,8,64,64]{3,2,1,0:T(8,128)S(1)} %get-tuple-element.198) | copy-start | bytes 3145732
  36.4 3.5 copy-start.6
  55.1 9.8 %copy-start.10 = (f32[8,8,64,64]{3,2,1,0:T(8,128)S(1)}, f32[8,8,64,64]{3,2,1,0:T(8,128)}, u32[]{:S(2)}) copy-start(f32[8,8,64,64]{3,2,1,0:T(8,128)} %fusion.110) | copy-start | bytes 3145732
  64.9 2.7 copy-start.13
  74.6 3.6 copy-start.16
  87.0 13.3 %copy-start.17 = (bf16[8,8,64,64]{2,3,1,0:T(8,128)(2,1)}, bf16[8,8,64,64]{2,3,1,0:T(8,128)(2,1)S(1)}, u32[]{:S(2)}) copy-start(bf16[8,8,64,64]{2,3,1,0:T(8,128)(2,1)S(1)} %copy.187) | copy-start | bytes 1572868
  87.0 5.5 %copy-start.12 = (f32[8,8,64,64]{3,2,1,0:T(8,128)S(1)}, f32[8,8,64,64]{3,2,1,0:T(8,128)}, u32[]{:S(2)}) copy-start(f32[8,8,64,64]{3,2,1,0:T(8,128)} %copy-done.11) | copy-start | bytes 3145732
  92.5 2.2 copy-start.21
  96.5 3.8 copy-start.2
  96.6 3.8 copy-start.5
  102.3 5.2 copy-start.14
  221.5 3.7 copy-start.3
  221.5 3.7 copy-start.7
  225.2 6.7 %copy-start.18 = (bf16[8,8,64,64]{2,3,1,0:T(8,128)(2,1)S(1)}, bf16[8,8,64,64]{2,3,1,0:T(8,128)(2,1)}, u32[]{:S(2)}) copy-start(bf16[8,8,64,64]{2,3,1,0:T(8,128)(2,1)} %copy-done.17) | copy-start | bytes 1572868
  225.2 6.7 %copy-start.20 = (f32[8,8,64,64]{3,2,1,0:T(8,128)S(1)}, f32[8,8,64,64]{3,2,1,0:T(8,128)}, u32[]{:S(2)}) copy-start(f32[8,8,64,64]{3,2,1,0:T(8,128)} %fusion.104) | copy-start | bytes 3145732
  225.2 6.7 %copy-start.22 = (f32[8,8,64,64]{2,3,1,0:T(8,128)S(1)}, f32[8,8,64,64]{2,3,1,0:T(8,128)}, u32[]{:S(2)}) copy-start(f32[8,8,64,64]{2,3,1,0:T(8,128)} %fusion.45) | copy-start | bytes 3145732
  248.8 53.0 %copy-start.23 = (bf16[128,2048]{1,0:T(8,128)(2,1)S(1)}, bf16[128,2048]{1,0:T(8,128)(2,1)}, u32[]{:S(2)}) copy-start(bf16[128,2048]{1,0:T(8,128)(2,1)} %param.35) | copy-start | bytes 1572868
  248.8 53.2 %copy-start.30 = (f32[2048]{0:T(1024)S(1)}, f32[2048]{0:T(1024)}, u32[]{:S(2)}) copy-start(f32[2048]{0:T(1024)} %param.36) | copy-start | bytes 24580
  248.9 139.9 %all-gather.4.cloned.1.call-start = ((), (), s32[]{:S(2)}) async-start(), calls=%async_computation.5 | async-start | bytes 7864320 | tf_op jit(solution)/shard_map/all_gather | solution.py:219
  344.1 122.5 %reduce-scatter.5.cloned.1.call-start = ((), (), s32[]{:S(2)}) async-start(), calls=%async_computation.6 | async-start | bytes 7864320 | tf_op jit(solution)/shard_map/reduce_scatter | solution.py:233
  407.6 64.3 %copy-start.34 = (f32[128,2]{0,1:T(2,128)S(1)}, f32[128,2]{0,1:T(2,128)}, u32[]{:S(2)}) copy-start(f32[128,2]{0,1:T(2,128)} %param.38) | copy-start | bytes 3076
  466.6 41.8 %all-to-all-start.1 = ((bf16[4,96,2048]{2,1,0:T(8,128)(2,1)}), bf16[4,96,2048]{2,1,0:T(8,128)(2,1)}, u32[]{:S(2)}, u32[]{:S(2)}) async-start(bf16[4,96,2048]{2,1,0:T(8,128)(2,1)} %reduce-scatter.5.cloned.1.call-done), calls=%async_computation.3 | async-start | bytes 3145728 | tf_op jit(solution)/shard_map/all_to_all | solution.py:236
  (7 other events, 11.1 us)
Sparse Core Ops, SparseCore 0:
  249.0 51.5 reduce-scatter.2
  344.2 44.4 all-gather.3
  407.7 58.8 reduce-scatter.4
where the time goes:
time: 537 us; the launch traced here: 529 us
  waiting for transfers between devices  189 us (35%)
  matrix products  150 us (28%)
  blocking collectives  87.8 us (16%)
  local copies, waits for them, and re-layouts  46.1 us (9%)
  other arithmetic  37.4 us (7%)
  between operations  14.3 us (3%)
    reduce_scatter x1, waiting for transfers between devices, local(): lax.psum_scatter(spread_rows.astype(jnp.bfloat16), 'tp', scatter_dimensio...  59 us
    reduce_scatter x1, waiting for transfers between devices, local(): lax.psum_scatter(jnp.dot(attention_result, output_weight_matrix, preferre...  48.6 us
    all_gather x2, blocking collectives, prefix_2(): gathered = jax.tree.map(lambda a: lax.all_gather(a, axis), part)  46.5 us
    all_gather x1, waiting for transfers between devices, local(): lax.all_gather(lax.all_to_all(outgoing, 'sp', split_axis=0, concat_axis=0...  44.6 us
    all_to_all x1, blocking collectives, local(): lax.all_to_all(outgoing, 'sp', split_axis=0, concat_axis=0, tiled=True)  41.3 us
    all_to_all x1, waiting for transfers between devices, local(): lax.all_to_all(summed, 'sp', split_axis=0, concat_axis=0, tiled=True)  36.3 us
    dot_general x10, matrix products, square_blocks(): return jnp.einsum('bhts,bhsu->bhtu', left, right, precision=PRECISE)  32.5 us
    dot_general x4, matrix products, pair_scores(): return jnp.einsum('bhtn,bhsn->bhts', left, right, precision=PRECISE)  23.9 us
  transfers between devices with their start and end apart: 4, of which 4 were waited for; matrix products, arithmetic and copies ran while one was open for 1% of the time, Pallas kernels for 0%

commit v1 on v0

v1 whole, which is shorter than its diff:
```python
import functools

import jax
import jax.numpy as jnp
from jax import lax
from jax.experimental import pallas as pl
from jax.experimental.pallas import tpu as pltpu
from jax.sharding import PartitionSpec as P


SPAN = 64


PRECISE = lax.Precision.HIGHEST
GROUP_EPS = 0.00064
NORM_EPS = 1e-06


def dot(left, right, contract=((1,), (0,))):
    return lax.dot_general(
        left.astype(jnp.bfloat16),
        right.astype(jnp.bfloat16),
        (contract, ((), ())),
        preferred_element_type=jnp.float32,
    )


NT = ((1,), (1,))
TN = ((0,), (0,))


def grid_pair(rows, cols):
    return (
        lax.broadcasted_iota(jnp.int32, (rows, cols), 0),
        lax.broadcasted_iota(jnp.int32, (rows, cols), 1),
    )


def head_sums(tensor, width):
    row, col = grid_pair(tensor.shape[1], tensor.shape[1])
    same = (row // width == col // width).astype(jnp.float32)
    return jnp.dot(tensor, same, precision=PRECISE, preferred_element_type=jnp.float32)


def chunk_kernel(
    recept_ref, key_ref, value_ref, decay_ref, rate_ref, offset_ref, bias_ref, rate_bias_ref,
    map_ref, own_ref, total_ref, *, width, pack
):
    group = pl.program_id(0)
    lanes = pack * width
    rows = pack * SPAN
    length = recept_ref.shape[0]
    blocks = length // SPAN
    decay = bias_ref[...] + decay_ref[...].astype(jnp.float32)
    decay_log = -jnp.exp(-jax.nn.softplus(-decay) - 0.5)
    row, col = grid_pair(offset_ref.shape[1], lanes)
    spread = (row == group * pack + col // width).astype(jnp.float32)
    decay_log = decay_log + jnp.dot(
        offset_ref[...], spread, precision=PRECISE, preferred_element_type=jnp.float32
    )
    rate = jax.nn.sigmoid(rate_bias_ref[...] + rate_ref[...].astype(jnp.float32))
    key = key_ref[...].astype(jnp.float32)
    unit_key = key * lax.rsqrt(head_sums(key * key, width) + NORM_EPS)
    recept = recept_ref[...].astype(jnp.float32)
    value = value_ref[...].astype(jnp.float32)

    row, col = grid_pair(SPAN, SPAN)
    ladder = (row >= col).astype(jnp.float32)
    row, col = grid_pair(rows, rows)
    same = row // SPAN == col // SPAN
    strict = same & (row > col)
    within = same & (row >= col)
    eye = (row == col).astype(jnp.float32)
    row, col = grid_pair(rows, lanes)
    mine = row // SPAN == col // width

    def stack(tensor):
        return jnp.where(mine, jnp.concatenate([tensor] * pack, axis=0), 0.0)

    def flat(tensor):
        total = tensor[:SPAN]
        for part in range(1, pack):
            total = total + tensor[part * SPAN : (part + 1) * SPAN]
        return total

    work = []
    for block in range(blocks):
        at = slice(block * SPAN, (block + 1) * SPAN)
        log = decay_log[at]
        cumul = jnp.dot(ladder, log, precision=PRECISE, preferred_element_type=jnp.float32)
        middle = cumul[SPAN // 2 - 1 : SPAN // 2]
        last = cumul[SPAN - 1 : SPAN]
        grow = jnp.exp(middle - cumul)
        remove = stack(-unit_key[at] * jnp.exp(cumul - log - middle))
        read = stack(recept[at] * jnp.exp(cumul - middle))
        write = stack(unit_key[at] * rate[at] * grow)
        keys = stack(key[at] * grow)
        values = stack(value[at])
        scores = dot(
            jnp.concatenate([remove, read], axis=0), jnp.concatenate([write, keys], axis=0), NT
        )
        closing = jnp.exp(last - middle)
        work.append(
            dict(
                remove=remove,
                read=read,
                values=values,
                write=write * closing,
                keys=keys * closing,
                opening=jnp.exp(middle),
                ending=jnp.exp(last),
                rw=jnp.where(strict, scores[:rows, :rows], 0.0),
                rk=jnp.where(strict, scores[:rows, rows:], 0.0),
                qw=jnp.where(within, scores[rows:, :rows], 0.0),
                qk=jnp.where(within, scores[rows:, rows:], 0.0),
            )
        )
    row, col = grid_pair(rows, rows)

    def joint(size):
        return (row // (2 * size) == col // (2 * size)) & (row // size > col // size)

    for w in work:
        w["inverse"] = eye + jnp.where(joint(1), w["rw"], 0.0)
        w["seen"] = dot(w["rk"], w["values"])
    size = 2
    while size < SPAN:
        pick = joint(size)
        for w in work:
            w["half"] = dot(jnp.where(pick, w["rw"], 0.0), w["inverse"])
        for w in work:
            w["inverse"] = w["inverse"] + dot(w["inverse"], w["half"])
        size *= 2
    for w in work:
        w["solved"] = dot(w["inverse"], jnp.concatenate([w["remove"], w["seen"]], axis=1))
        w["own"] = dot(w["qk"], w["values"])
    for w in work:
        answer = dot(w["qw"], w["solved"])
        w["map"] = flat(w["read"] + answer[:, :lanes]) * w["opening"]
        w["own"] = flat(w["own"] + answer[:, lanes:])
        inv_remove = w["solved"][:, :lanes] * w["opening"]
        inv_value = w["solved"][:, lanes:]
        w["move"] = dot(inv_remove, w["write"], TN)
        w["added"] = dot(
            jnp.concatenate([inv_value, w["values"]], axis=0),
            jnp.concatenate([w["write"], w["keys"]], axis=0),
            TN,
        )
    row, col = grid_pair(lanes, lanes)
    transit = (row == col).astype(jnp.float32)
    state = jnp.zeros((lanes, lanes), jnp.float32)
    for block, w in enumerate(work):
        at = slice(block * SPAN, (block + 1) * SPAN)
        both = jnp.concatenate([transit, state], axis=0)
        seen = dot(w["map"], both, NT)
        map_ref[at, :] = seen[:, :lanes].astype(map_ref.dtype)
        own_ref[at, :] = w["own"] + seen[:, lanes:]
        both = both * w["ending"] + dot(both, w["move"])
        transit = both[:lanes]
        state = both[lanes:] + w["added"]

    def compact(tensor):
        total = tensor[:width]
        for part in range(1, pack):
            total = total + tensor[part * width : (part + 1) * width]
        return total

    total_ref[0, :width, :] = compact(transit).astype(total_ref.dtype)
    total_ref[0, width:, :] = compact(state).astype(total_ref.dtype)


def read_kernel(
    place_ref, map_ref, own_ref, totals_ref, recept_ref, key_ref, value_ref, gate_ref, gain_ref,
    self_ref, out_ref, enter_ref, *, width, pack
):
    lanes = pack * width
    row, col = grid_pair(lanes, lanes)
    same = row // width == col // width

    def expand(tensor):
        return jnp.where(same, jnp.concatenate([tensor] * pack, axis=0), 0.0)

    enter_ref[...] = jnp.zeros((lanes, lanes), jnp.float32)

    @pl.loop(0, place_ref[0])
    def _(lap):
        both = totals_ref[lap, 0].astype(jnp.float32)
        enter_ref[...] = dot(enter_ref[...], expand(both[:width])) + expand(both[width:])

    readout = own_ref[...] + dot(map_ref[...], enter_ref[...], NT)
    center = head_sums(readout, width) * (1.0 / width)
    shifted = readout - center
    spread = head_sums(shifted * shifted, width) * (1.0 / width)
    normalized = shifted * lax.rsqrt(spread + GROUP_EPS) * gain_ref[...]
    recept = recept_ref[...].astype(jnp.float32)
    key = key_ref[...].astype(jnp.float32)
    self_term = head_sums(recept * key * self_ref[...], width)
    merged = normalized + self_term * value_ref[...].astype(jnp.float32)
    out_ref[...] = (merged * gate_ref[...].astype(jnp.float32)).astype(jnp.bfloat16)


def mixer(
    recept,
    key_input,
    value_input,
    decay_input_part,
    correction_rate_input,
    head_decay_offset,
    decay_fixed_bias,
    correction_rate_bias,
):
    length, channels = recept.shape
    heads = head_decay_offset.shape[1]
    width = channels // heads
    pack = 2 if heads % 2 == 0 else 1
    lanes = pack * width
    groups = heads // pack
    long = pl.BlockSpec((length, lanes), lambda g: (0, g))
    flat = pl.BlockSpec((1, lanes), lambda g: (0, g))
    readmap, own, total = pl.pallas_call(
        functools.partial(chunk_kernel, width=width, pack=pack),
        grid=(groups,),
        in_specs=[long] * 5 + [pl.BlockSpec((length, heads), lambda g: (0, 0)), flat, flat],
        out_specs=[long, long, pl.BlockSpec((1, 2 * width, lanes), lambda g: (g, 0, 0))],
        out_shape=[
            jax.ShapeDtypeStruct((length, channels), jnp.bfloat16),
            jax.ShapeDtypeStruct((length, channels), jnp.float32),
            jax.ShapeDtypeStruct((groups, 2 * width, lanes), jnp.bfloat16),
        ],
        compiler_params=pltpu.CompilerParams(vmem_limit_bytes=56 * 2**20),
        cost_estimate=pl.CostEstimate(
            flops=40_000_000_000, bytes_accessed=4 * length * channels, transcendentals=0
        ),
        name="chunk_phase",
    )(
        recept, key_input, value_input, decay_input_part, correction_rate_input,
        head_decay_offset, decay_fixed_bias[None], correction_rate_bias[None],
    )
    return readmap, own, total, long, flat, width, pack, groups


def readout_phase(phase, place, totals, recept, key_input, value_input, gate, gain, self_weight):
    readmap, own, total, long, flat, width, pack, groups = phase
    del total
    count = totals.shape[0]
    lanes = pack * width
    return pl.pallas_call(
        functools.partial(read_kernel, width=width, pack=pack),
        grid=(groups,),
        in_specs=[
            pl.BlockSpec(memory_space=pltpu.SMEM),
            long,
            long,
            pl.BlockSpec((count, 1, 2 * width, lanes), lambda g: (0, g, 0, 0)),
            long,
            long,
            long,
            long,
            flat,
            flat,
        ],
        out_specs=long,
        out_shape=jax.ShapeDtypeStruct(own.shape, jnp.bfloat16),
        scratch_shapes=[pltpu.VMEM((lanes, lanes), jnp.float32)],
        compiler_params=pltpu.CompilerParams(vmem_limit_bytes=40 * 2**20),
        name="read_phase",
    )(place, readmap, own, totals, recept, key_input, value_input, gate, gain[None], self_weight[None])


def local(
    recept,
    key_input,
    value_input,
    output_gate_input,
    decay_input_part,
    correction_rate_input,
    head_decay_offset,
    decay_fixed_bias,
    correction_rate_bias,
    head_norm_gain,
    self_term_weight,
    output_weight_matrix,
    residual,
    feedforward_norm_gain,
    routed_expert_index,
    routed_expert_weight,
    gate_weight_experts,
    up_weight_experts,
    down_weight_experts,
):
    experts = gate_weight_experts.shape[0] * lax.axis_size("sp")
    few = experts <= 2 * routed_expert_index.shape[1]
    if few:
        gate_all = lax.all_gather(gate_weight_experts[0], "sp")
        up_all = lax.all_gather(up_weight_experts[0], "sp")
        down_all = lax.all_gather(down_weight_experts[0], "sp")
        named = routed_expert_index[:, :, None] == jnp.arange(experts, dtype=jnp.int32)
        route = jnp.sum(jnp.where(named, routed_expert_weight[:, :, None], 0.0), axis=1)
        route_all = lax.all_gather(route, "tp", axis=0, tiled=True)
    phase = mixer(
        recept,
        key_input,
        value_input,
        decay_input_part,
        correction_rate_input,
        head_decay_offset,
        decay_fixed_bias,
        correction_rate_bias,
    )
    totals = lax.all_gather(phase[2], "sp")
    place = lax.axis_index("sp").astype(jnp.int32).reshape(1)
    attention_result = readout_phase(
        phase,
        place,
        totals,
        recept,
        key_input,
        value_input,
        output_gate_input,
        head_norm_gain,
        self_term_weight,
    )
    partial = jnp.dot(attention_result, output_weight_matrix, preferred_element_type=jnp.float32)
    proj = lax.psum_scatter(
        partial.astype(jnp.bfloat16), "tp", scatter_dimension=0, tiled=True
    )
    stream = residual.astype(jnp.float32) + proj.astype(jnp.float32)
    ffn_in = (
        stream
        * lax.rsqrt(jnp.mean(stream * stream, axis=-1, keepdims=True) + NORM_EPS)
        * feedforward_norm_gain
    ).astype(jnp.bfloat16)
    local_rows = ffn_in.shape[0]
    top_count = routed_expert_index.shape[1]
    experts = gate_weight_experts.shape[0] * lax.axis_size("sp")
    if few:
        rows = lax.all_gather(ffn_in, "tp", axis=0, tiled=True)
        pieces = []
        for e in range(experts):
            gated = jnp.dot(rows, gate_all[e], preferred_element_type=jnp.float32)
            upward = jnp.dot(rows, up_all[e], preferred_element_type=jnp.float32)
            scaled = jax.nn.silu(gated) * upward * route_all[:, e : e + 1]
            pieces.append(scaled.astype(jnp.bfloat16))
        hidden = jnp.concatenate(pieces, axis=1)
        down = down_all.reshape(-1, down_all.shape[-1])
        result = jnp.dot(hidden, down, preferred_element_type=jnp.float32)
        summed = lax.psum_scatter(
            result.astype(jnp.bfloat16), "tp", scatter_dimension=0, tiled=True
        )
        return (stream + summed.astype(jnp.float32)).astype(jnp.bfloat16)
    capacity = max(2, 3 * local_rows // experts)
    flat_ids = routed_expert_index.reshape(-1)
    hits = (flat_ids[:, None] == jnp.arange(experts, dtype=jnp.int32)[None, :]).astype(jnp.int32)
    earlier_hits = jnp.cumsum(hits, axis=0) - hits
    slot_index = jnp.sum(earlier_hits * hits, axis=1)
    target = flat_ids * capacity + slot_index
    places = (target[:, None] == jnp.arange(experts * capacity, dtype=jnp.int32)[None, :]).astype(
        jnp.bfloat16
    )
    places = jnp.sum(places.reshape(local_rows, top_count, experts * capacity), axis=1)
    outgoing = jnp.einsum("rs,rd->sd", places, ffn_in, preferred_element_type=jnp.float32)
    outgoing = outgoing.astype(jnp.bfloat16).reshape(experts, capacity, ffn_in.shape[1])
    incoming = lax.all_gather(
        lax.all_to_all(outgoing, "sp", split_axis=0, concat_axis=0, tiled=True),
        "tp",
        axis=0,
        tiled=True,
    )
    flat = incoming.reshape(-1, incoming.shape[-1])
    gated = jnp.dot(flat, gate_weight_experts[0], preferred_element_type=jnp.float32)
    upward = jnp.dot(flat, up_weight_experts[0], preferred_element_type=jnp.float32)
    hidden = (jax.nn.silu(gated) * upward).astype(jnp.bfloat16)
    result = jnp.dot(hidden, down_weight_experts[0], preferred_element_type=jnp.float32)
    spread_rows = lax.optimization_barrier(
        result.astype(jnp.bfloat16).reshape(incoming.shape)
    ).astype(jnp.float32)
    summed = lax.psum_scatter(
        spread_rows.astype(jnp.bfloat16), "tp", scatter_dimension=0, tiled=True
    )
    expert_out = lax.all_to_all(summed, "sp", split_axis=0, concat_axis=0, tiled=True)
    table = expert_out.reshape(experts * capacity, expert_out.shape[-1])
    fetched = jnp.take(table, target, axis=0).astype(jnp.float32)
    weighted = jnp.sum(
        fetched.reshape(local_rows, top_count, -1) * routed_expert_weight[:, :, None], axis=1
    )
    return (stream + weighted).astype(jnp.bfloat16)


def solution(mesh):
    return jax.shard_map(
        local,
        mesh=mesh,
        in_specs=(
            P(("grp", "sp"), "tp"),
            P(("grp", "sp"), "tp"),
            P(("grp", "sp"), "tp"),
            P(("grp", "sp"), "tp"),
            P(("grp", "sp"), "tp"),
            P(("grp", "sp"), "tp"),
            P(("grp", "sp"), "tp"),
            P("tp"),
            P("tp"),
            P("tp"),
            P("tp"),
            P("tp", None),
            P(("grp", "sp", "tp"), None),
            P(),
            P(("grp", "sp", "tp"), None),
            P(("grp", "sp", "tp"), None),
            P("sp", None, "tp"),
            P("sp", None, "tp"),
            P("sp", "tp", None),
        ),
        out_specs=P(("grp", "sp", "tp"), None),
        check_vma=False,
    )
```

time: 537 us -> 378 us (0.70); the launches traced: 529 us -> 378 us
  matrix products: 150 us -> 26.7 us
  waiting for transfers between devices: 189 us -> 273 us
  blocking collectives: 87.8 us -> 22.9 us
  local copies, waits for them, and re-layouts: 46.1 us -> 8.17 us
  other arithmetic: 37.4 us -> 5.45 us
  Pallas kernels: 0 us -> 25.9 us
    all_gather x1 -> x4, waiting for transfers between devices: 44.6 us -> 207 us  [the longest x1 72.6 us: local(): up_all = lax.all_gather(up_weight_experts[0], 'sp')]
    dot_general x44 -> x9, matrix products: 146 us -> 24.1 us  [the longest x4 9.44 us: local(): gated = jnp.dot(rows, gate_all[e], preferred_element_type=jnp.float32)]
    reduce_scatter x2, waiting for transfers between devices: 108 us -> 64 us  [the longest x1 34.2 us: local(): lax.psum_scatter(partial.astype(jnp.bfloat16), 'tp', scatter_dimension=0,...]
    all_to_all x1 -> x0, blocking collectives: 41.3 us -> none  [local(): lax.all_to_all(outgoing, 'sp', split_axis=0, concat_axis=0, tiled=True)]
    all_to_all x1 -> x0, waiting for transfers between devices: 36.3 us -> none  [local(): lax.all_to_all(summed, 'sp', split_axis=0, concat_axis=0, tiled=True)]
    pallas_call x0 -> x2, Pallas kernels: none -> 25.9 us  [the longest x1 20.9 us: mixer(): pl.pallas_call(functools.partial(chunk_kernel, width=width, pack=pack), g...]
    all_gather x2, blocking collectives: 46.5 us -> 22.9 us  [the longest x1 17.6 us: local(): totals = lax.all_gather(phase[2], 'sp')]
    reduce_sum x5 -> x1, other arithmetic: 9.97 us -> 0.01 us  [local(): jnp.sum(jnp.where(named, routed_expert_weight[:, :, None], 0.0), axis=1)]
  transfers between devices with their start and end apart: 4 -> 6, of which waited for: 4 -> 6; matrix products, arithmetic and copies ran while one was open for 1% -> 6% of each run, Pallas kernels for 0% -> 0%
where the time goes in v1:
time: 378 us
  waiting for transfers between devices  273 us (72%)
  matrix products  26.7 us (7%)
  Pallas kernels  25.9 us (7%)
  blocking collectives  22.9 us (6%)
  between operations  15.2 us (4%)
  local copies, waits for them, and re-layouts  8.17 us (2%)
  other arithmetic  5.45 us (1%)
    all_gather x1, waiting for transfers between devices, local(): up_all = lax.all_gather(up_weight_experts[0], 'sp')  72.6 us
    all_gather x1, waiting for transfers between devices, local(): down_all = lax.all_gather(down_weight_experts[0], 'sp')  71.2 us
    all_gather x1, waiting for transfers between devices, local(): gate_all = lax.all_gather(gate_weight_experts[0], 'sp')  41.1 us
    reduce_scatter x1, waiting for transfers between devices, local(): lax.psum_scatter(partial.astype(jnp.bfloat16), 'tp', scatter_dimension=0,...  34.2 us
    reduce_scatter x1, waiting for transfers between devices, local(): lax.psum_scatter(result.astype(jnp.bfloat16), 'tp', scatter_dimension=0,...  29.8 us
    all_gather x1, waiting for transfers between devices, local(): rows = lax.all_gather(ffn_in, 'tp', axis=0, tiled=True)  22.4 us
    pallas_call x1, Pallas kernels, mixer(): pl.pallas_call(functools.partial(chunk_kernel, width=width, pack=pack), g...  20.9 us
    all_gather x1, blocking collectives, local(): totals = lax.all_gather(phase[2], 'sp')  17.6 us
  transfers between devices with their start and end apart: 6, of which 6 were waited for; matrix products, arithmetic and copies ran while one was open for 6% of the time, Pallas kernels for 0%

profile of v1, /device:TPU:0, one launch (start us, length us, event | category | flops | bytes accessed | tf_op | source)
XLA Modules:
  0.0 377.5 jit_solution(6947583505343719280)
XLA Ops:
  7.4 1.7 copy.29.offset_ref
  9.1 20.9 %chunk_phase.1 = (bf16[512,512]{1,0:T(8,128)(2,1)}, f32[512,512]{1,0:T(8,128)}, bf16[4,128,128]{2,1,0:T(8,128)(2,1)}) custom-call(bf16[512,512]{1,0:T(8,128)(2,1)} %recept_ref.3, bf16[512,512]{1,0:T(8,128)(2,1)} %key_ref.3, bf16[512,512]{1,0:T(8,128)(2,1)} %value_ref.3, bf16[512,512]{1,0:T(8,128)(2,1)} %decay_ref.1, bf16[512,512]{1,0:T(8,128)(2,1)} %rate_ref.1, ...), custom_call_target="tpu_custom_call" | custom-call | flops 40000000000 | bytes 1048576 | tf_op jit(solution)/shard_map/chunk_phase/pallas_call | solution.py:220
  29.9 17.6 %all-gather = bf16[16,128,128]{2,1,0:T(8,128)(2,1)S(1)} all-gather(bf16[4,128,128]{2,1,0:T(8,128)(2,1)} %get-tuple-element.10), channel_id=2, replica_groups=mesh['grp'=2,'sp'=4,'tp'=4] {'sp'}, dimensions={0}, use_global_device_ids=true | all-gather | bytes 655360 | tf_op jit(solution)/shard_map/all_gather | solution.py:310
  47.5 1.2 copy-done.1
  48.7 1.0 copy-done.3
  49.8 1.0 copy-done.4
  50.8 1.0 copy-done.5
  51.9 1.0 copy-done.6
  52.9 5.0 %read_phase.1 = bf16[512,512]{1,0:T(8,128)(2,1)S(1)} custom-call(s32[1]{0:T(128)} %bitcast.place_ref, bf16[512,512]{1,0:T(8,128)(2,1)S(1)} %copy-done.6, f32[512,512]{1,0:T(8,128)S(1)} %copy-done.1, bf16[4,4,128,128]{3,2,1,0:T(8,128)(2,1)S(1)} %bitcast.46, bf16[512,512]{1,0:T(8,128)(2,1)S(1)} %copy-done.2, bf16[512,512]{1,0:T(8,128)(2,1)S(1)} %copy-done.3, ...), custom_call_target="tpu_custom_call" | custom-call | tf_op jit(solution)/shard_map/read_phase/pallas_call | solution.py:247
  57.9 2.6 convolution_convert_fusion.1
  60.6 0.5 all-gather.8.cloned.1.call-update
  61.2 34.2 %reduce-scatter.3.cloned.1.call-done = bf16[128,2048]{1,0:T(8,128)(2,1)} async-done(((bf16[512,2048]{1,0:T(8,128)(2,1)}), bf16[128,2048]{1,0:T(8,128)(2,1)}) %reduce-scatter.3.cloned.1.call-update) | async-done | bytes 524304 | tf_op jit(solution)/shard_map/reduce_scatter | solution.py:324
  95.4 1.3 multiply_reduce_fusion
  96.7 2.1 multiply_convert_fusion
  99.4 0.7 all-gather.12.cloned.1.call-update
  100.2 5.4 %all_gather.26 = f32[512,4]{0,1:T(4,128)S(1)} all-gather(f32[128,4]{0,1:T(4,128)S(1)} %select_reduce_fusion), channel_id=1, replica_groups=mesh['grp'=2,'sp'=4,'tp'=4] {'tp'}, dimensions={0}, use_global_device_ids=true | all-gather | bytes 10240 | tf_op jit(solution)/shard_map/all_gather | solution.py:299
  105.5 41.1 %all-gather.8.cloned.1.call-done = bf16[4,2048,256]{2,1,0:T(8,128)(2,1)} async-done(((bf16[1,2048,256]{2,1,0:T(8,128)(2,1)}), bf16[4,2048,256]{2,1,0:T(8,128)(2,1)}) %all-gather.8.cloned.1.call-update) | async-done | bytes 4194320 | tf_op jit(solution)/shard_map/all_gather | solution.py:294
  146.7 22.4 %all-gather.6.cloned.1.call-done = bf16[512,2048]{1,0:T(8,128)(2,1)} async-done(((bf16[128,2048]{1,0:T(8,128)(2,1)}), bf16[512,2048]{1,0:T(8,128)(2,1)}) %all-gather.6.cloned.1.call-update) | async-done | bytes 2097168 | tf_op jit(solution)/shard_map/all_gather | solution.py:337
  169.1 3.6 fusion.11
  172.6 3.6 fusion.10
  176.2 1.6 fusion.9
  177.8 0.7 fusion.8
  178.5 72.6 %all-gather.10.cloned.1.call-done = bf16[4,2048,256]{2,1,0:T(8,128)(2,1)} async-done(((bf16[1,2048,256]{2,1,0:T(8,128)(2,1)}), bf16[4,2048,256]{2,1,0:T(8,128)(2,1)}) %all-gather.10.cloned.1.call-update) | async-done | bytes 4194320 | tf_op jit(solution)/shard_map/all_gather | solution.py:295
  251.1 2.9 fusion.4
  254.4 0.7 copy-done.17
  255.1 2.6 fusion.5
  257.7 1.5 fusion.6
  259.2 1.5 fusion.7
  260.7 71.2 %all-gather.12.cloned.1.call-done = bf16[4,256,2048]{2,1,0:T(8,128)(2,1)} async-done(((bf16[1,256,2048]{2,1,0:T(8,128)(2,1)}), bf16[4,256,2048]{2,1,0:T(8,128)(2,1)}) %all-gather.12.cloned.1.call-update) | async-done | bytes 4194320 | tf_op jit(solution)/shard_map/all_gather | solution.py:296
  331.8 6.2 %convolution_convert_fusion = bf16[512,2048]{1,0:T(8,128)(2,1)} fusion(bf16[1024,2048]{1,0:T(8,128)(2,1)} %bitcast.53, bf16[512,256]{0,1:T(8,128)(2,1)} %fusion.7, bf16[512,256]{0,1:T(8,128)(2,1)} %fusion.6, bf16[512,256]{0,1:T(8,128)(2,1)} %fusion.5, bf16[512,256]{0,1:T(8,128)(2,1)S(1)} %fusion.4), kind=kOutput, calls=%fused_computation | convolution fusion | flops 2152726528 | bytes 7340032 | tf_op jit(solution)/shard_map/dot_general | solution.py:346
  338.0 29.8 %reduce-scatter.5.cloned.1.call-done = bf16[128,2048]{1,0:T(8,128)(2,1)} async-done(((bf16[512,2048]{1,0:T(8,128)(2,1)}), bf16[128,2048]{1,0:T(8,128)(2,1)}) %reduce-scatter.5.cloned.1.call-update) | async-done | bytes 524304 | tf_op jit(solution)/shard_map/reduce_scatter | solution.py:347
  367.9 2.1 add_convert_fusion
  (45 shorter events, 1.2 us)
Async XLA Ops:
  7.4 50.6 %copy-start = (bf16[512,2048]{1,0:T(8,128)(2,1)S(1)}, bf16[512,2048]{1,0:T(8,128)(2,1)}, u32[]{:S(2)}) copy-start(bf16[512,2048]{1,0:T(8,128)(2,1)} %param.30) | copy-start | bytes 6291460
  7.4 88.0 %reduce-scatter.3.cloned.1.call-start = ((), (), s32[]{:S(2)}) async-start(), calls=%async_computation.2 | async-start | bytes 2621440 | tf_op jit(solution)/shard_map/reduce_scatter | solution.py:324
  9.1 38.4 %copy-start.2 = (bf16[512,512]{1,0:T(8,128)(2,1)S(1)}, bf16[512,512]{1,0:T(8,128)(2,1)}, u32[]{:S(2)}) copy-start(bf16[512,512]{1,0:T(8,128)(2,1)} %recept_ref.3) | copy-start | bytes 1572868
  9.1 38.4 %copy-start.7 = (f32[512]{0:T(512)S(1)}, f32[512]{0:T(512)}, u32[]{:S(2)}) copy-start(f32[512]{0:T(512)} %param.28) | copy-start | bytes 6148
  9.1 38.4 %copy-start.8 = (f32[512]{0:T(512)S(1)}, f32[512]{0:T(512)}, u32[]{:S(2)}) copy-start(f32[512]{0:T(512)} %param.29) | copy-start | bytes 6148
  47.5 1.2 copy-start.1
  48.7 1.0 copy-start.3
  49.8 1.0 copy-start.4
  50.8 1.0 copy-start.5
  51.9 1.0 copy-start.6
  60.5 34.8 %copy-start.9 = (bf16[128,2048]{1,0:T(8,128)(2,1)S(1)}, bf16[128,2048]{1,0:T(8,128)(2,1)}, u32[]{:S(2)}) copy-start(bf16[128,2048]{1,0:T(8,128)(2,1)} %param.31) | copy-start | bytes 1572868
  60.5 36.1 %copy-start.11 = (f32[2048]{0:T(1024)S(1)}, f32[2048]{0:T(1024)}, u32[]{:S(2)}) copy-start(f32[2048]{0:T(1024)} %param.32) | copy-start | bytes 24580
  60.5 86.1 %all-gather.8.cloned.1.call-start = ((), (), s32[]{:S(2)}) async-start(), calls=%async_computation.4 | async-start | bytes 5242880 | tf_op jit(solution)/shard_map/all_gather | solution.py:294
  61.1 107.9 %all-gather.6.cloned.1.call-start = ((), (), s32[]{:S(2)}) async-start(), calls=%async_computation.3 | async-start | bytes 2621440 | tf_op jit(solution)/shard_map/all_gather | solution.py:337
  96.7 3.5 copy-start.12
  96.7 3.5 copy-start.13
  98.8 152.4 %all-gather.10.cloned.1.call-start = ((), (), s32[]{:S(2)}) async-start(), calls=%async_computation.5 | async-start | bytes 5242880 | tf_op jit(solution)/shard_map/all_gather | solution.py:295
  99.3 232.5 %all-gather.12.cloned.1.call-start = ((), (), s32[]{:S(2)}) async-start(), calls=%async_computation.6 | async-start | bytes 5242880 | tf_op jit(solution)/shard_map/all_gather | solution.py:296
  100.1 267.8 %reduce-scatter.5.cloned.1.call-start = ((), (), s32[]{:S(2)}) async-start(), calls=%async_computation.7 | async-start | bytes 2621440 | tf_op jit(solution)/shard_map/reduce_scatter | solution.py:347
  169.1 7.1 %copy-start.14 = (bf16[4,2048,256]{2,1,0:T(8,128)(2,1)S(1)}, bf16[4,2048,256]{2,1,0:T(8,128)(2,1)}, u32[]{:S(2)}) copy-start(bf16[4,2048,256]{2,1,0:T(8,128)(2,1)} %all-gather.8.cloned.1.call-done) | copy-start | bytes 12582916
  172.6 3.6 copy-start.16
  251.1 3.3 copy-start.15
  251.1 4.0 %copy-start.17 = (bf16[512,2048]{1,0:T(8,128)(2,1)S(1)}, bf16[512,2048]{1,0:T(8,128)(2,1)}, u32[]{:S(2)}) copy-start(bf16[512,2048]{1,0:T(8,128)(2,1)} %all-gather.6.cloned.1.call-done) | copy-start | bytes 6291460
  255.1 2.6 copy-start.18
  338.0 29.9 %copy-start.10 = (bf16[128,2048]{1,0:T(8,128)(2,1)S(1)}, bf16[128,2048]{1,0:T(8,128)(2,1)}, u32[]{:S(2)}) copy-start(bf16[128,2048]{1,0:T(8,128)(2,1)} %reduce-scatter.3.cloned.1.call-done) | copy-start | bytes 1572868
Sparse Core Ops, SparseCore 0:
  60.7 34.6 reduce-scatter.2
  338.2 29.6 reduce-scatter.4
Sparse Core Ops, SparseCore 1:
  62.6 84.0 all-gather.7
  148.1 20.9 all-gather.5
  170.5 80.6 all-gather.9
  252.7 79.1 all-gather.11

commit v2 on v1

--- a/solution.py
+++ b/solution.py
@@ -17,12 +17,15 @@
 
 
 def dot(left, right, contract=((1,), (0,))):
-    return lax.dot_general(
-        left.astype(jnp.bfloat16),
-        right.astype(jnp.bfloat16),
-        (contract, ((), ())),
-        preferred_element_type=jnp.float32,
-    )
+    def once(a, b):
+        return lax.dot_general(
+            a, b, (contract, ((), ())), preferred_element_type=jnp.float32
+        )
+
+    left_high, right_high = left.astype(jnp.bfloat16), right.astype(jnp.bfloat16)
+    left_low = (left - left_high.astype(jnp.float32)).astype(jnp.bfloat16)
+    right_low = (right - right_high.astype(jnp.float32)).astype(jnp.bfloat16)
+    return once(left_high, right_high) + once(left_high, right_low) + once(left_low, right_high)
 
 
 NT = ((1,), (1,))
@@ -223,7 +226,7 @@
         in_specs=[long] * 5 + [pl.BlockSpec((length, heads), lambda g: (0, 0)), flat, flat],
         out_specs=[long, long, pl.BlockSpec((1, 2 * width, lanes), lambda g: (g, 0, 0))],
         out_shape=[
-            jax.ShapeDtypeStruct((length, channels), jnp.bfloat16),
+            jax.ShapeDtypeStruct((length, channels), jnp.float32),
             jax.ShapeDtypeStruct((length, channels), jnp.float32),
             jax.ShapeDtypeStruct((groups, 2 * width, lanes), jnp.bfloat16),
         ],
@@ -289,11 +292,30 @@
     down_weight_experts,
 ):
     experts = gate_weight_experts.shape[0] * lax.axis_size("sp")
-    few = experts <= 2 * routed_expert_index.shape[1]
+    few = (
+        experts <= 2 * routed_expert_index.shape[1]
+        and experts == lax.axis_size("sp")
+        and lax.axis_size("grp") == 2
+        and gate_weight_experts.shape[2] % 256 == 0
+    )
     if few:
-        gate_all = lax.all_gather(gate_weight_experts[0], "sp")
-        up_all = lax.all_gather(up_weight_experts[0], "sp")
-        down_all = lax.all_gather(down_weight_experts[0], "sp")
+        half = gate_weight_experts.shape[2] // 2
+        group = lax.axis_index("grp")
+        place = lax.axis_index("sp")
+
+        def fetch(weight, axis):
+            near = lax.dynamic_slice_in_dim(weight, group * half, half, axis)
+            far = lax.dynamic_slice_in_dim(weight, (1 - group) * half, half, axis)
+            gathered = lax.all_gather(near, "sp")
+            blocks = [gathered[e] for e in range(experts)] + [far]
+            for step in range(1, experts):
+                chosen = lax.dynamic_index_in_dim(gathered, (place + step) % experts, 0, False)
+                blocks.append(lax.ppermute(chosen, "grp", [(0, 1), (1, 0)]))
+            return gathered, blocks
+
+        _, gate_blocks = fetch(gate_weight_experts[0], 1)
+        _, up_blocks = fetch(up_weight_experts[0], 1)
+        down_all, down_blocks = fetch(down_weight_experts[0], 0)
         named = routed_expert_index[:, :, None] == jnp.arange(experts, dtype=jnp.int32)
         route = jnp.sum(jnp.where(named, routed_expert_weight[:, :, None], 0.0), axis=1)
         route_all = lax.all_gather(route, "tp", axis=0, tiled=True)
@@ -336,13 +358,15 @@
     if few:
         rows = lax.all_gather(ffn_in, "tp", axis=0, tiled=True)
         pieces = []
-        for e in range(experts):
-            gated = jnp.dot(rows, gate_all[e], preferred_element_type=jnp.float32)
-            upward = jnp.dot(rows, up_all[e], preferred_element_type=jnp.float32)
-            scaled = jax.nn.silu(gated) * upward * route_all[:, e : e + 1]
-            pieces.append(scaled.astype(jnp.bfloat16))
+        for at in range(2 * experts):
+            gated = jnp.dot(rows, gate_blocks[at], preferred_element_type=jnp.float32)
+            upward = jnp.dot(rows, up_blocks[at], preferred_element_type=jnp.float32)
+            expert = at if at < experts else (place + at - experts) % experts
+            mine = jnp.arange(experts, dtype=jnp.int32)[None, :] == expert
+            share = jnp.sum(jnp.where(mine, route_all, 0.0), axis=1, keepdims=True)
+            pieces.append((jax.nn.silu(gated) * upward * share).astype(jnp.bfloat16))
         hidden = jnp.concatenate(pieces, axis=1)
-        down = down_all.reshape(-1, down_all.shape[-1])
+        down = jnp.concatenate([down_all.reshape(-1, rows.shape[1])] + down_blocks[experts:], axis=0)
         result = jnp.dot(hidden, down, preferred_element_type=jnp.float32)
         summed = lax.psum_scatter(
             result.astype(jnp.bfloat16), "tp", scatter_dimension=0, tiled=True

time: 378 us -> 347 us (0.918)
  waiting for transfers between devices: 273 us -> 196 us
  local copies, waits for them, and re-layouts: 8.17 us -> 24.4 us
  Pallas kernels: 25.9 us -> 40.1 us
  starting transfers between devices: 0.21 us -> 10.8 us
    all_gather x3, waiting for transfers between devices: 185 us -> 90.9 us  [fetch(): gathered = lax.all_gather(near, 'sp')]
    ppermute x0 -> x9, waiting for transfers between devices: none -> 45.6 us  [fetch(): blocks.append(lax.ppermute(chosen, 'grp', [(0, 1), (1, 0)]))]
    all_gather x1, waiting for transfers between devices: 22.4 us -> 0.01 us  [local(): rows = lax.all_gather(ffn_in, 'tp', axis=0, tiled=True)]
    pallas_call x1, Pallas kernels: 20.9 us -> 34.2 us  [mixer(): pl.pallas_call(functools.partial(chunk_kernel, width=width, pack=pack), g...]
    ppermute x0 -> x9, starting transfers between devices: none -> 10.6 us  [fetch(): blocks.append(lax.ppermute(chosen, 'grp', [(0, 1), (1, 0)]))]
    squeeze x0 -> x3, local copies, waits for them, and re-layouts: none -> 7.7 us  [fetch(): lax.dynamic_index_in_dim(gathered, (place + step) % experts, 0, False)]
    dynamic_slice x0 -> x3, local copies, waits for them, and re-layouts: none -> 5.72 us  [fetch(): near = lax.dynamic_slice_in_dim(weight, group * half, half, axis)]
    reduce_scatter x1, waiting for transfers between devices: 34.2 us -> 29.2 us  [local(): lax.psum_scatter(partial.astype(jnp.bfloat16), 'tp', scatter_dimension=0,...]
  transfers between devices with their start and end apart: 6 -> 15, of which waited for: 6 -> 9; matrix products, arithmetic and copies ran while one was open for 6% -> 13% of each run, Pallas kernels for 0% -> 0%
where the time goes in v2:
time: 347 us; the launch traced here: 346 us
  waiting for transfers between devices  196 us (56%)
  Pallas kernels  40.1 us (12%)
  matrix products  30 us (9%)
  local copies, waits for them, and re-layouts  24.4 us (7%)
  blocking collectives  22.9 us (7%)
  between operations  15.5 us (4%)
  starting transfers between devices  10.8 us (3%)
  other arithmetic  5.59 us (2%)
    all_gather x3, waiting for transfers between devices, fetch(): gathered = lax.all_gather(near, 'sp')  90.9 us
    ppermute x9, waiting for transfers between devices, fetch(): blocks.append(lax.ppermute(chosen, 'grp', [(0, 1), (1, 0)]))  45.6 us
    pallas_call x1, Pallas kernels, mixer(): pl.pallas_call(functools.partial(chunk_kernel, width=width, pack=pack), g...  34.2 us
    reduce_scatter x1, waiting for transfers between devices, local(): lax.psum_scatter(result.astype(jnp.bfloat16), 'tp', scatter_dimension=0,...  30.5 us
    reduce_scatter x1, waiting for transfers between devices, local(): lax.psum_scatter(partial.astype(jnp.bfloat16), 'tp', scatter_dimension=0,...  29.2 us
    all_gather x1, blocking collectives, local(): totals = lax.all_gather(phase[2], 'sp')  17.6 us
    dot_general x8, matrix products, local(): gated = jnp.dot(rows, gate_blocks[at], preferred_element_type=jnp.float32)  12.8 us
    ppermute x9, starting transfers between devices, fetch(): blocks.append(lax.ppermute(chosen, 'grp', [(0, 1), (1, 0)]))  10.6 us
  transfers between devices with their start and end apart: 15, of which 9 were waited for; matrix products, arithmetic and copies ran while one was open for 13% of the time, Pallas kernels for 0%

profile of v2, /device:TPU:0, one launch (start us, length us, event | category | flops | bytes accessed | tf_op | source)
XLA Modules:
  0.0 345.7 jit_solution(11332525940388538579)
XLA Ops:
  7.4 1.7 copy.26.offset_ref
  9.1 34.2 %chunk_phase.1 = (f32[512,512]{1,0:T(8,128)}, f32[512,512]{1,0:T(8,128)}, bf16[4,128,128]{2,1,0:T(8,128)(2,1)}) custom-call(bf16[512,512]{1,0:T(8,128)(2,1)} %recept_ref.3, bf16[512,512]{1,0:T(8,128)(2,1)} %key_ref.3, bf16[512,512]{1,0:T(8,128)(2,1)} %value_ref.3, bf16[512,512]{1,0:T(8,128)(2,1)} %decay_ref.1, bf16[512,512]{1,0:T(8,128)(2,1)} %rate_ref.1, ...), custom_call_target="tpu_custom_call" | custom-call | flops 40000000000 | bytes 1048576 | tf_op jit(solution)/shard_map/chunk_phase/pallas_call | solution.py:223
  43.4 17.6 %all-gather = bf16[16,128,128]{2,1,0:T(8,128)(2,1)S(1)} all-gather(bf16[4,128,128]{2,1,0:T(8,128)(2,1)} %get-tuple-element.10), channel_id=2, replica_groups=mesh['grp'=2,'sp'=4,'tp'=4] {'sp'}, dimensions={0}, use_global_device_ids=true | all-gather | bytes 655360 | tf_op jit(solution)/shard_map/all_gather | solution.py:332
  63.4 5.9 %read_phase.1 = bf16[512,512]{1,0:T(8,128)(2,1)S(1)} custom-call(s32[1]{0:T(128)} %bitcast.place_ref, f32[512,512]{1,0:T(8,128)S(1)} %copy-done.1, f32[512,512]{1,0:T(8,128)S(1)} %copy-done.2, bf16[4,4,128,128]{3,2,1,0:T(8,128)(2,1)S(1)} %bitcast.87, bf16[512,512]{1,0:T(8,128)(2,1)S(1)} %copy-done.3, bf16[512,512]{1,0:T(8,128)(2,1)S(1)} %copy-done.4, ...), custom_call_target="tpu_custom_call" | custom-call | tf_op jit(solution)/shard_map/read_phase/pallas_call | solution.py:250
  69.3 2.6 convolution_convert_fusion.1
  72.0 1.9 constant_dynamic-slice_fusion.2
  73.9 1.9 constant_dynamic-slice_fusion
  75.9 1.9 constant_dynamic-slice_fusion.1
  77.9 29.2 %reduce-scatter.3.cloned.1.call-done = bf16[128,2048]{1,0:T(8,128)(2,1)} async-done(((bf16[512,2048]{1,0:T(8,128)(2,1)}), bf16[128,2048]{1,0:T(8,128)(2,1)}) %reduce-scatter.3.cloned.1.call-update) | async-done | bytes 524304 | tf_op jit(solution)/shard_map/reduce_scatter | solution.py:346
  108.4 2.0 multiply_convert_fusion
  110.7 5.4 %all_gather.29 = f32[512,4]{0,1:T(4,128)S(1)} all-gather(f32[128,4]{0,1:T(4,128)S(1)} %select_reduce_fusion.8), channel_id=1, replica_groups=mesh['grp'=2,'sp'=4,'tp'=4] {'tp'}, dimensions={0}, use_global_device_ids=true | all-gather | bytes 10240 | tf_op jit(solution)/shard_map/all_gather | solution.py:321
  116.2 7.2 %all-gather.8.cloned.1.call-done = bf16[4,2048,128]{2,1,0:T(8,128)(2,1)} async-done(((bf16[1,2048,128]{2,1,0:T(8,128)(2,1)}), bf16[4,2048,128]{2,1,0:T(8,128)(2,1)}) %all-gather.8.cloned.1.call-update) | async-done | bytes 2097168 | tf_op jit(solution)/shard_map/all_gather | solution.py:309
  123.4 2.4 dynamic-slice_bitcast_fusion.4
  127.3 41.9 %all-gather.12.cloned.1.call-done = bf16[4,128,2048]{2,1,0:T(8,128)(2,1)} async-done(((bf16[1,128,2048]{2,1,0:T(8,128)(2,1)}), bf16[4,128,2048]{2,1,0:T(8,128)(2,1)}) %all-gather.12.cloned.1.call-update) | async-done | bytes 2097168 | tf_op jit(solution)/shard_map/all_gather | solution.py:309
  169.2 2.5 dynamic-slice_bitcast_fusion
  173.2 41.8 %all-gather.10.cloned.1.call-done = bf16[4,2048,128]{2,1,0:T(8,128)(2,1)} async-done(((bf16[1,2048,128]{2,1,0:T(8,128)(2,1)}), bf16[4,2048,128]{2,1,0:T(8,128)(2,1)}) %all-gather.10.cloned.1.call-update) | async-done | bytes 2097168 | tf_op jit(solution)/shard_map/all_gather | solution.py:309
  215.0 2.7 dynamic-slice_bitcast_fusion.3
  224.2 1.9 constant_dynamic-update-slice_fusion.2
  226.1 17.8 %collective-permute-done.7 = bf16[128,2048]{1,0:T(8,128)(2,1)S(1)} collective-permute-done((bf16[128,2048]{1,0:T(8,128)(2,1)S(1)}, bf16[128,2048]{1,0:T(8,128)(2,1)S(1)}, u32[]{:S(2)}, u32[]{:S(2)}) %collective-permute-start.7) | collective-permute-done | bytes 524320 | tf_op jit(solution)/shard_map/ppermute | solution.py:313
  246.3 8.9 %collective-permute-done.8 = bf16[128,2048]{1,0:T(8,128)(2,1)S(1)} collective-permute-done((bf16[128,2048]{1,0:T(8,128)(2,1)S(1)}, bf16[128,2048]{1,0:T(8,128)(2,1)S(1)}, u32[]{:S(2)}, u32[]{:S(2)}) %collective-permute-start.8) | collective-permute-done | bytes 524320 | tf_op jit(solution)/shard_map/ppermute | solution.py:313
  257.5 2.6 fusion.18
  260.2 2.0 fusion.17
  264.6 1.9 fusion.29
  272.4 1.9 fusion.24
  274.3 1.9 fusion.30
  276.1 12.9 %collective-permute-done.4 = bf16[2048,128]{1,0:T(8,128)(2,1)} collective-permute-done((bf16[2048,128]{1,0:T(8,128)(2,1)S(1)}, bf16[2048,128]{1,0:T(8,128)(2,1)}, u32[]{:S(2)}, u32[]{:S(2)}) %collective-permute-start.4) | collective-permute-done | bytes 524320 | tf_op jit(solution)/shard_map/ppermute | solution.py:313
  289.0 1.9 fusion.31
  290.9 1.9 fusion.25
  292.8 5.9 %collective-permute-done.5 = bf16[2048,128]{1,0:T(8,128)(2,1)S(1)} collective-permute-done((bf16[2048,128]{1,0:T(8,128)(2,1)S(1)}, bf16[2048,128]{1,0:T(8,128)(2,1)S(1)}, u32[]{:S(2)}, u32[]{:S(2)}) %collective-permute-start.5) | collective-permute-done | bytes 524320 | tf_op jit(solution)/shard_map/ppermute | solution.py:313
  299.6 5.9 %convolution_convert_fusion = bf16[512,2048]{1,0:T(8,128)(2,1)} fusion(bf16[512,1024]{0,1:T(8,128)(2,1)S(1)} %fusion.26, bf16[1024,2048]{1,0:T(8,128)(2,1)} %constant_dynamic-update-slice_fusion), kind=kOutput, calls=%fused_computation | convolution fusion | flops 2148532224 | bytes 7340032 | tf_op jit(solution)/shard_map/dot_general | solution.py:370
  305.5 30.5 %reduce-scatter.5.cloned.1.call-done = bf16[128,2048]{1,0:T(8,128)(2,1)} async-done(((bf16[512,2048]{1,0:T(8,128)(2,1)}), bf16[128,2048]{1,0:T(8,128)(2,1)}) %reduce-scatter.5.cloned.1.call-update) | async-done | bytes 524304 | tf_op jit(solution)/shard_map/reduce_scatter | solution.py:371
  336.0 2.1 add_convert_fusion
  (96 shorter events, 27.3 us)
Async XLA Ops:
  7.4 61.9 %copy-start = (bf16[512,2048]{1,0:T(8,128)(2,1)S(1)}, bf16[512,2048]{1,0:T(8,128)(2,1)}, u32[]{:S(2)}) copy-start(bf16[512,2048]{1,0:T(8,128)(2,1)} %param.30) | copy-start | bytes 6291460
  7.4 99.7 %reduce-scatter.3.cloned.1.call-start = ((), (), s32[]{:S(2)}) async-start(), calls=%async_computation.2 | async-start | bytes 2621440 | tf_op jit(solution)/shard_map/reduce_scatter | solution.py:346
  9.1 51.9 %copy-start.3 = (bf16[512,512]{1,0:T(8,128)(2,1)S(1)}, bf16[512,512]{1,0:T(8,128)(2,1)}, u32[]{:S(2)}) copy-start(bf16[512,512]{1,0:T(8,128)(2,1)} %recept_ref.3) | copy-start | bytes 1572868
  9.1 51.9 %copy-start.4 = (bf16[512,512]{1,0:T(8,128)(2,1)S(1)}, bf16[512,512]{1,0:T(8,128)(2,1)}, u32[]{:S(2)}) copy-start(bf16[512,512]{1,0:T(8,128)(2,1)} %key_ref.3) | copy-start | bytes 1572868
  9.1 51.9 %copy-start.5 = (bf16[512,512]{1,0:T(8,128)(2,1)S(1)}, bf16[512,512]{1,0:T(8,128)(2,1)}, u32[]{:S(2)}) copy-start(bf16[512,512]{1,0:T(8,128)(2,1)} %value_ref.3) | copy-start | bytes 1572868
  9.1 51.9 %copy-start.6 = (bf16[512,512]{1,0:T(8,128)(2,1)S(1)}, bf16[512,512]{1,0:T(8,128)(2,1)}, u32[]{:S(2)}) copy-start(bf16[512,512]{1,0:T(8,128)(2,1)} %gate_ref.1) | copy-start | bytes 1572868
  9.1 51.9 %copy-start.7 = (f32[512]{0:T(512)S(1)}, f32[512]{0:T(512)}, u32[]{:S(2)}) copy-start(f32[512]{0:T(512)} %param.28) | copy-start | bytes 6148
  9.1 51.9 %copy-start.8 = (f32[512]{0:T(512)S(1)}, f32[512]{0:T(512)}, u32[]{:S(2)}) copy-start(f32[512]{0:T(512)} %param.29) | copy-start | bytes 6148
  71.9 51.5 %all-gather.8.cloned.1.call-start = ((), (), s32[]{:S(2)}) async-start(), calls=%async_computation.4 | async-start | bytes 2621440 | tf_op jit(solution)/shard_map/all_gather | solution.py:309
  73.8 33.3 %copy-start.12 = (bf16[128,2048]{1,0:T(8,128)(2,1)S(1)}, bf16[128,2048]{1,0:T(8,128)(2,1)}, u32[]{:S(2)}) copy-start(bf16[128,2048]{1,0:T(8,128)(2,1)} %param.31) | copy-start | bytes 1572868
  73.9 34.6 %copy-start.21 = (f32[2048]{0:T(1024)S(1)}, f32[2048]{0:T(1024)}, u32[]{:S(2)}) copy-start(f32[2048]{0:T(1024)} %param.32) | copy-start | bytes 24580
  73.9 95.3 %all-gather.12.cloned.1.call-start = ((), (), s32[]{:S(2)}) async-start(), calls=%async_computation.6 | async-start | bytes 2621440 | tf_op jit(solution)/shard_map/all_gather | solution.py:309
  75.9 139.1 %all-gather.10.cloned.1.call-start = ((), (), s32[]{:S(2)}) async-start(), calls=%async_computation.5 | async-start | bytes 2621440 | tf_op jit(solution)/shard_map/all_gather | solution.py:309
  77.9 32.8 %copy-start.22 = (f32[128,2]{0,1:T(2,128)S(1)}, f32[128,2]{0,1:T(2,128)}, u32[]{:S(2)}) copy-start(f32[128,2]{0,1:T(2,128)} %param.34) | copy-start | bytes 3076
  77.9 32.8 %copy-start.23 = (s32[128,2]{0,1:T(2,128)S(1)}, s32[128,2]{0,1:T(2,128)}, u32[]{:S(2)}) copy-start(s32[128,2]{0,1:T(2,128)} %param.33) | copy-start | bytes 3076
  77.9 179.6 %all-gather.6.cloned.1.call-start = ((), (), s32[]{:S(2)}) async-start(), calls=%async_computation.3 | async-start | bytes 2621440 | tf_op jit(solution)/shard_map/all_gather | solution.py:359
  110.5 225.5 %reduce-scatter.5.cloned.1.call-start = ((), (), s32[]{:S(2)}) async-start(), calls=%async_computation.7 | async-start | bytes 2621440 | tf_op jit(solution)/shard_map/reduce_scatter | solution.py:371
  125.8 138.1 %collective-permute-start = (bf16[2048,128]{1,0:T(8,128)(2,1)}, bf16[2048,128]{1,0:T(8,128)(2,1)}, u32[]{:S(2)}, u32[]{:S(2)}) collective-permute-start(bf16[2048,128]{1,0:T(8,128)(2,1)} %get-tuple-element.24), channel_id=1, source_target_pairs={{0,16},{16,0},{1,17},{17,1},{2,18},{18,2},{3,19},{19,3},{4,20},{20... | collective-permute-start | bytes 1572872 | tf_op jit(solution)/shard_map/ppermute | solution.py:313
  171.7 51.9 %collective-permute-start.6 = (bf16[128,2048]{1,0:T(8,128)(2,1)}, bf16[128,2048]{1,0:T(8,128)(2,1)}, u32[]{:S(2)}, u32[]{:S(2)}) collective-permute-start(bf16[128,2048]{1,0:T(8,128)(2,1)} %get-tuple-element.21), channel_id=1, source_target_pairs={{0,16},{16,0},{1,17},{17,1},{2,18},{18,2},{3,19},{19,3},{4,20},{20... | collective-permute-start | bytes 1572872 | tf_op jit(solution)/shard_map/ppermute | solution.py:313
  215.0 4.2 %copy-start.19 = (bf16[128,2048]{1,0:T(8,128)(2,1)S(1)}, bf16[128,2048]{1,0:T(8,128)(2,1)}, u32[]{:S(2)}) copy-start(bf16[128,2048]{1,0:T(8,128)(2,1)} %get-tuple-element.20) | copy-start | bytes 1572868
  215.0 4.8 %copy-start.10 = (bf16[4,128,2048]{2,1,0:T(8,128)(2,1)S(1)}, bf16[4,128,2048]{2,1,0:T(8,128)(2,1)}, u32[]{:S(2)}) copy-start(bf16[4,128,2048]{2,1,0:T(8,128)(2,1)} %all-gather.12.cloned.1.call-done) | copy-start | bytes 6291460
  217.7 54.6 %collective-permute-start.1 = (bf16[2048,128]{1,0:T(8,128)(2,1)}, bf16[2048,128]{1,0:T(8,128)(2,1)}, u32[]{:S(2)}, u32[]{:S(2)}) collective-permute-start(bf16[2048,128]{1,0:T(8,128)(2,1)} %get-tuple-element.27), channel_id=1, source_target_pairs={{0,16},{16,0},{1,17},{17,1},{2,18},{18,2},{3,19},{19,3},{4,20},{20... | collective-permute-start | bytes 1572872 | tf_op jit(solution)/shard_map/ppermute | solution.py:313
  219.2 24.8 %collective-permute-start.7 = (bf16[128,2048]{1,0:T(8,128)(2,1)S(1)}, bf16[128,2048]{1,0:T(8,128)(2,1)S(1)}, u32[]{:S(2)}, u32[]{:S(2)}) collective-permute-start(bf16[128,2048]{1,0:T(8,128)(2,1)S(1)} %copy-done.19), channel_id=1, source_target_pairs={{0,16},{16,0},{1,17},{17,1},{2,18},{18,2},{3,19},{19,3},{4,20},{20... | collective-permute-start | bytes 1572872 | tf_op jit(solution)/shard_map/ppermute | solution.py:313
  219.7 3.0 copy-start.15
  221.2 34.0 %collective-permute-start.8 = (bf16[128,2048]{1,0:T(8,128)(2,1)S(1)}, bf16[128,2048]{1,0:T(8,128)(2,1)S(1)}, u32[]{:S(2)}, u32[]{:S(2)}) collective-permute-start(bf16[128,2048]{1,0:T(8,128)(2,1)S(1)} %copy-done.18), channel_id=1, source_target_pairs={{0,16},{16,0},{1,17},{17,1},{2,18},{18,2},{3,19},{19,3},{4,20},{20... | collective-permute-start | bytes 1572872 | tf_op jit(solution)/shard_map/ppermute | solution.py:313
  223.5 50.7 %collective-permute-start.2 = (bf16[2048,128]{1,0:T(8,128)(2,1)}, bf16[2048,128]{1,0:T(8,128)(2,1)}, u32[]{:S(2)}, u32[]{:S(2)}) collective-permute-start(bf16[2048,128]{1,0:T(8,128)(2,1)} %get-tuple-element.23), channel_id=1, source_target_pairs={{0,16},{16,0},{1,17},{17,1},{2,18},{18,2},{3,19},{19,3},{4,20},{20... | collective-permute-start | bytes 1572872 | tf_op jit(solution)/shard_map/ppermute | solution.py:313
  244.0 46.9 %collective-permute-start.3 = (bf16[2048,128]{1,0:T(8,128)(2,1)}, bf16[2048,128]{1,0:T(8,128)(2,1)}, u32[]{:S(2)}, u32[]{:S(2)}) collective-permute-start(bf16[2048,128]{1,0:T(8,128)(2,1)} %get-tuple-element.26), channel_id=1, source_target_pairs={{0,16},{16,0},{1,17},{17,1},{2,18},{18,2},{3,19},{19,3},{4,20},{20... | collective-permute-start | bytes 1572872 | tf_op jit(solution)/shard_map/ppermute | solution.py:313
  255.2 33.8 %collective-permute-start.4 = (bf16[2048,128]{1,0:T(8,128)(2,1)S(1)}, bf16[2048,128]{1,0:T(8,128)(2,1)}, u32[]{:S(2)}, u32[]{:S(2)}) collective-permute-start(bf16[2048,128]{1,0:T(8,128)(2,1)S(1)} %get-tuple-element.22), channel_id=1, source_target_pairs={{0,16},{16,0},{1,17},{17,1},{2,18},{18,2},{3,19},{19,3},{4,20},{20... | collective-permute-start | bytes 1572872 | tf_op jit(solution)/shard_map/ppermute | solution.py:313
  257.5 2.7 copy-start.9
  263.9 2.6 copy-start.14
  264.1 34.6 %collective-permute-start.5 = (bf16[2048,128]{1,0:T(8,128)(2,1)S(1)}, bf16[2048,128]{1,0:T(8,128)(2,1)S(1)}, u32[]{:S(2)}, u32[]{:S(2)}) collective-permute-start(bf16[2048,128]{1,0:T(8,128)(2,1)S(1)} %copy-done.17), channel_id=1, source_target_pairs={{0,16},{16,0},{1,17},{17,1},{2,18},{18,2},{3,19},{19,3},{4,20},{20... | collective-permute-start | bytes 1572872 | tf_op jit(solution)/shard_map/ppermute | solution.py:313
  305.5 30.5 %copy-start.13 = (bf16[128,2048]{1,0:T(8,128)(2,1)S(1)}, bf16[128,2048]{1,0:T(8,128)(2,1)}, u32[]{:S(2)}) copy-start(bf16[128,2048]{1,0:T(8,128)(2,1)} %reduce-scatter.3.cloned.1.call-done) | copy-start | bytes 1572868
  (7 other events, 9.5 us)
Sparse Core Ops, SparseCore 0:
  72.0 35.0 reduce-scatter.2
  305.6 30.2 reduce-scatter.4
Sparse Core Ops, SparseCore 1:
  74.0 49.4 all-gather.7
  124.8 44.3 all-gather.11
  170.6 44.3 all-gather.9
  216.5 21.2 all-gather.5
